TPU v7x, 32 devices: a whole 2x2x4 slice. The times are simulated.
32 devices in a mesh: ep: 8 (over z, x), tp: 4 (over y, core).
Axes of the slice: x: 2, y: 2, z: 4, core: 2. Of those that a mesh axis runs over, the one named last changes fastest.
Arguments:
- tokens: bfloat16 [512, 2048], P('ep', 'tp')
- norm_gain: float32 [2048], P('tp'), may hold values from 0.1 to 1.9
- expert_ids: int32 [512, 4], P('ep'), may hold values from 0 to 7, all different within a row; in each aligned block of 64 rows (0 to 63, 64 to 127, ...) at most 64 rows name the same one
- route_weights: float32 [512, 4], P('ep'), may hold values from 0.1 to 1
- gate_proj: bfloat16 [8, 2048, 2048], P('ep', None, 'tp'), may hold values from -0.5 to 0.5
- up_proj: bfloat16 [8, 2048, 2048], P('ep', None, 'tp'), may hold values from -0.5 to 0.5
- down_proj: bfloat16 [8, 2048, 2048], P('ep', 'tp')
- final_gain: float32 [2048], P('tp'), may hold values from 0.1 to 1.9
Outputs:
- layer_output: bfloat16 [512, 2048], P('ep', 'tp')
Inputs may be any that keep to these rules, and one draw needn't show every extreme that they name: `expert_ids`: each row names 4 different experts. Within the 64 rows of one device no expert is named by more than 64 rows, a bound that some block reaches.
All inputs are finite; a program needn't handle non-finite values.
Results may differ from a plain program's by a relative error of at most 0.017.
Values may be sent and summed in bfloat16 or wider, within the bound.
A program may use at most 64 MiB of HBM per device.

v0:
```python
import jax
import jax.numpy as jnp
from jax import lax
from jax.sharding import PartitionSpec as P

EPSILON = 1e-05
CLAMP_LIMIT = 7.0
SIGMOID_SLOPE = 1.702


def slot_tables(id_block, gate_block, targets, capacity):
    matches = (id_block[:, :, None] == targets[None, None, :]).astype(jnp.int32)
    per_token = jnp.sum(matches, axis=1)
    earlier = jnp.cumsum(per_token, axis=0) - per_token
    slot_places = lax.broadcasted_iota(jnp.int32, (1, 1, capacity), 2)
    selector = (
        per_token[:, :, None] * (earlier[:, :, None] == slot_places).astype(jnp.int32)
    ).astype(jnp.float32)
    weights = jnp.sum(gate_block[:, :, None] * matches.astype(jnp.float32), axis=1)
    return (selector, weights)


def expert_partial(flat_rows, gate_proj, up_proj, down_proj):
    gate_pre = jnp.minimum(
        jnp.dot(flat_rows, gate_proj[0], preferred_element_type=jnp.float32), CLAMP_LIMIT
    )
    up_pre = jnp.clip(
        jnp.dot(flat_rows, up_proj[0], preferred_element_type=jnp.float32),
        -CLAMP_LIMIT,
        CLAMP_LIMIT,
    )
    activated = ((up_pre + 1.0) * gate_pre * jax.nn.sigmoid(SIGMOID_SLOPE * gate_pre)).astype(
        jnp.bfloat16
    )
    return jnp.dot(activated, down_proj[0], preferred_element_type=jnp.float32)


def local(tokens, norm_gain, expert_ids, route_weights, gate_proj, up_proj, down_proj, final_gain):
    tok_rows, local_width = tokens.shape
    choose_count = expert_ids.shape[1]
    model_width = local_width * lax.axis_size("tp")
    expert_count = lax.axis_size("ep")
    capacity = min(tok_rows, 2 * tok_rows * choose_count // expert_count)
    input_rows = tokens.astype(jnp.float32)
    squares = lax.psum(jnp.sum(input_rows * input_rows, axis=1), "tp")
    normed = (
        input_rows * lax.rsqrt(squares / model_width + EPSILON)[:, None] * norm_gain[None, :]
    ).astype(jnp.bfloat16)
    targets = lax.iota(jnp.int32, expert_count)
    selector, weights = slot_tables(expert_ids, route_weights, targets, capacity)
    picker = selector.astype(jnp.bfloat16)
    outbound = jnp.einsum("tec,td->ecd", picker, normed, preferred_element_type=jnp.float32).astype(
        jnp.bfloat16
    )
    received = lax.all_gather(
        lax.all_to_all(outbound, "ep", split_axis=0, concat_axis=0, tiled=True),
        "tp",
        axis=2,
        tiled=True,
    )
    flat_rows = received.reshape(-1, model_width)
    partial_value = expert_partial(flat_rows, gate_proj, up_proj, down_proj)
    summed = lax.psum_scatter(
        partial_value.astype(jnp.bfloat16), "tp", scatter_dimension=1, tiled=True
    )
    expert_out = summed.reshape(received.shape[0], received.shape[1], local_width)
    returned = lax.all_to_all(expert_out, "ep", split_axis=0, concat_axis=0, tiled=True)
    mixture = jnp.einsum(
        "tec,ecd->td", selector * weights[:, :, None], returned.astype(jnp.float32)
    )
    squares_out = lax.psum(jnp.sum(mixture * mixture, axis=1), "tp")
    return (
        mixture * lax.rsqrt(squares_out / model_width + EPSILON)[:, None] * final_gain[None, :]
    ).astype(jnp.bfloat16)


def solution(mesh):
    placed = (
        P("ep", "tp"),
        P("tp"),
        P("ep", None),
        P("ep", None),
        P("ep", None, "tp"),
        P("ep", None, "tp"),
        P("ep", "tp", None),
        P("tp"),
    )
    return jax.shard_map(
        local, mesh=mesh, in_specs=placed, out_specs=P("ep", "tp"), check_vma=False
    )
```

profile of v0, /device:TPU:0, one launch (start us, length us, event | category | flops | bytes accessed | tf_op | source)
XLA Modules:
  0.0 133.9 jit_solution(14307365750482966474)
XLA Ops:
  6.5 0.0 copy-start
  6.5 0.0 all-gather.2.cloned.1.call-start
  6.5 0.8 convert_reduce_fusion
  7.4 0.1 copy.14
  7.5 0.1 reduce_window_sum.11
  7.6 0.1 copy.16
  7.6 1.0 fusion.32
  8.6 8.4 %psum.14 = f32[64]{0:T(128)S(1)} all-reduce(f32[64]{0:T(128)S(1)} %fusion.32), channel_id=1, replica_groups=mesh['ep'=8,'tp'=4] {'tp'}, use_global_device_ids=true, to_apply=%region_4.5 | all-reduce | flops 64 | bytes 512 | tf_op jit(solution)/shard_map/psum | solution.py:45
  17.0 1.4 %convolution_convert_fusion.1 = bf16[8,64,512]{2,1,0:T(8,128)(2,1)S(1)} fusion(s32[64,8]{0,1:T(8,128)S(1)} %convert_reduce_fusion, s32[64,8]{0,1:T(8,128)S(1)} %copy.16, bf16[64,512]{1,0:T(8,128)(2,1)} %param.8, f32[512]{0:T(512)} %param.9, f32[64]{0:T(128)S(1)} %add_rsqrt_fusion.1), kind=kOutput, calls=%fused_computation.12 | convolution fusion | flops 34078720 | bytes 596224 | tf_op jit(solution)/shard_map/tec,td->ecd/dot_general | solution.py:52
  18.4 19.0 %all_to_all.10 = bf16[8,64,512]{2,1,0:T(8,128)(2,1)} all-to-all(bf16[8,64,512]{2,1,0:T(8,128)(2,1)S(1)} %convolution_convert_fusion.1), channel_id=1, replica_groups=mesh['ep'=8,'tp'=4] {'ep'}, dimensions={0} | all-to-all | bytes 1048576 | tf_op jit(solution)/shard_map/all_to_all | solution.py:56
  37.4 0.0 all-gather.2.cloned.1.call-update
  37.4 0.0 reduce-scatter.2.cloned.1.call-start
  37.4 21.8 %all-gather.2.cloned.1.call-done = bf16[8,64,2048]{2,1,0:T(8,128)(2,1)} async-done(((bf16[8,64,512]{2,1,0:T(8,128)(2,1)}), bf16[8,64,2048]{2,1,0:T(8,128)(2,1)}) %all-gather.2.cloned.1.call-update) | async-done | bytes 2097168 | tf_op jit(solution)/shard_map/all_gather | solution.py:55
  59.2 3.5 %fusion.8 = f32[512,512]{1,0:T(8,128)S(1)} fusion(bf16[512,2048]{1,0:T(8,128)(2,1)} %bitcast.34, bf16[1,2048,512]{2,1,0:T(8,128)(2,1)} %param.12), kind=kOutput, calls=%fused_computation.7 | convolution fusion | flops 1074003968 | bytes 5242880 | tf_op jit(solution)/shard_map/dot_general | solution.py:25
  62.7 0.0 copy-done
  62.7 6.0 %convolution_convert_fusion = bf16[512,2048]{1,0:T(8,128)(2,1)} fusion(bf16[1,512,2048]{2,1,0:T(8,128)(2,1)S(1)} %copy-done, f32[512,512]{1,0:T(8,128)S(1)} %fusion.8, bf16[512,2048]{1,0:T(8,128)(2,1)} %bitcast.35, bf16[1,2048,512]{2,1,0:T(8,128)(2,1)} %param.13), kind=kOutput, calls=%fused_computation | convolution fusion | flops 2150891520 | bytes 9437184 | tf_op jit(solution)/shard_map/dot_general | solution.py:35
  68.7 0.0 copy-start.1
  68.7 0.0 copy-start.3
  68.7 0.0 copy-start.2
  68.7 0.0 reduce-scatter.2.cloned.1.call-update
  68.8 31.3 %reduce-scatter.2.cloned.1.call-done = bf16[512,512]{1,0:T(8,128)(2,1)} async-done(((bf16[512,2048]{1,0:T(8,128)(2,1)}), bf16[512,512]{1,0:T(8,128)(2,1)}) %reduce-scatter.2.cloned.1.call-update) | async-done | bytes 524304 | tf_op jit(solution)/shard_map/reduce_scatter | solution.py:63
  100.1 5.5 %all-to-all-start.1 = ((bf16[8,64,512]{2,1,0:T(8,128)(2,1)}), bf16[8,64,512]{2,1,0:T(8,128)(2,1)S(1)}, u32[]{:S(2)}, u32[]{:S(2)}) async-start(bf16[8,64,512]{2,1,0:T(8,128)(2,1)} %bitcast.33), calls=%async_computation.2 | async-start | bytes 1048576 | tf_op jit(solution)/shard_map/all_to_all | solution.py:67
  105.6 0.0 copy-done.1
  105.6 0.0 copy-done.3
  105.6 14.3 %all-to-all-done.1 = bf16[8,64,512]{2,1,0:T(8,128)(2,1)S(1)} async-done(((bf16[8,64,512]{2,1,0:T(8,128)(2,1)}), bf16[8,64,512]{2,1,0:T(8,128)(2,1)S(1)}, u32[]{:S(2)}, u32[]{:S(2)}) %all-to-all-start.1) | async-done | bytes 524320 | tf_op jit(solution)/shard_map/all_to_all | solution.py:67
  119.9 0.5 multiply_reduce_fusion
  120.4 5.9 %psum.15 = f32[64]{0:T(128)S(1)} all-reduce(f32[64]{0:T(128)S(1)} %get-tuple-element.5), channel_id=1, replica_groups=mesh['ep'=8,'tp'=4] {'tp'}, use_global_device_ids=true, to_apply=%region_7.8 | all-reduce | flops 64 | bytes 512 | tf_op jit(solution)/shard_map/psum | solution.py:71
  126.4 0.0 copy-done.2
  126.4 0.7 multiply_convert_fusion
  (4 shorter events, 0.0 us)
Async XLA Ops:
  6.5 56.2 %copy-start = (bf16[1,512,2048]{2,1,0:T(8,128)(2,1)S(1)}, bf16[1,512,2048]{2,1,0:T(8,128)(2,1)}, u32[]{:S(2)}) copy-start(bf16[1,512,2048]{2,1,0:T(8,128)(2,1)} %param.14) | copy-start | bytes 6291460
  6.5 52.7 %all-gather.2.cloned.1.call-start = ((), (), s32[]{:S(2)}) async-start(), calls=%async_computation.3 | async-start | bytes 2621440 | tf_op jit(solution)/shard_map/all_gather | solution.py:55
  37.4 62.7 %reduce-scatter.2.cloned.1.call-start = ((), (), s32[]{:S(2)}) async-start(), calls=%async_computation.4 | async-start | bytes 2621440 | tf_op jit(solution)/shard_map/reduce_scatter | solution.py:63
  68.7 36.9 %copy-start.1 = (s32[64,4]{0,1:T(4,128)S(1)}, s32[64,4]{0,1:T(4,128)}, u32[]{:S(2)}) copy-start(s32[64,4]{0,1:T(4,128)} %param.10) | copy-start | bytes 3076
  68.7 36.9 %copy-start.3 = (f32[64,4]{0,1:T(4,128)S(1)}, f32[64,4]{0,1:T(4,128)}, u32[]{:S(2)}) copy-start(f32[64,4]{0,1:T(4,128)} %param.11) | copy-start | bytes 3076
  68.7 57.6 %copy-start.2 = (f32[512]{0:T(512)S(1)}, f32[512]{0:T(512)}, u32[]{:S(2)}) copy-start(f32[512]{0:T(512)} %param.15) | copy-start | bytes 6148
  100.1 19.8 %all-to-all-start.1 = ((bf16[8,64,512]{2,1,0:T(8,128)(2,1)}), bf16[8,64,512]{2,1,0:T(8,128)(2,1)S(1)}, u32[]{:S(2)}, u32[]{:S(2)}) async-start(bf16[8,64,512]{2,1,0:T(8,128)(2,1)} %bitcast.33), calls=%async_computation.2 | async-start | bytes 1048576 | tf_op jit(solution)/shard_map/all_to_all | solution.py:67
Sparse Core Ops, SparseCore 0:
  37.5 21.6 all-gather.1
  68.9 31.1 reduce-scatter.1
where the time goes:
time: 134 us
  waiting for transfers between devices  67.4 us (50%)
  blocking collectives  33.3 us (25%)
  between operations  13.5 us (10%)
  matrix products  11.4 us (9%)
  starting transfers between devices  5.56 us (4%)
  other arithmetic  2.65 us (2%)
    reduce_scatter x1, waiting for transfers between devices, local(): lax.psum_scatter(partial_value.astype(jnp.bfloat16), 'tp', scatter_dimens...  31.3 us
    all_gather x1, waiting for transfers between devices, local(): lax.all_gather(lax.all_to_all(outbound, 'ep', split_axis=0, concat_axis=0...  21.8 us
    all_to_all x1, blocking collectives, local(): lax.all_to_all(outbound, 'ep', split_axis=0, concat_axis=0, tiled=True)  19 us
    all_to_all x1, waiting for transfers between devices, local(): lax.all_to_all(expert_out, 'ep', split_axis=0, concat_axis=0, tiled=True)  14.3 us
    psum x1, blocking collectives, local(): squares = lax.psum(jnp.sum(input_rows * input_rows, axis=1), 'tp')  8.4 us
    dot_general x1, matrix products, expert_partial(): return jnp.dot(activated, down_proj[0], preferred_element_type=jnp.float32)  6.02 us
    psum x1, blocking collectives, local(): squares_out = lax.psum(jnp.sum(mixture * mixture, axis=1), 'tp')  5.94 us
    all_to_all x1, starting transfers between devices, local(): lax.all_to_all(expert_out, 'ep', split_axis=0, concat_axis=0, tiled=True)  5.51 us
  transfers between devices with their start and end apart: 3, of which 3 were waited for; matrix products, arithmetic and copies ran while one was open for 0% of the time, Pallas kernels for 0%

commit v1 on v0

--- a/solution.py
+++ b/solution.py
@@ -1,10 +1,16 @@
+import functools
+
 import jax
 import jax.numpy as jnp
 from jax import lax
+from jax.experimental import pallas as pl
+from jax.experimental.pallas import tpu as pltpu
 from jax.sharding import PartitionSpec as P
 
 EPSILON = 1e-05
 CLAMP_LIMIT = 7.0
+MESH = pl.DeviceIdType.MESH
+PER_GROUP = 17
 SIGMOID_SLOPE = 1.702
 
 
@@ -74,6 +80,360 @@
     ).astype(jnp.bfloat16)
 
 
+def fused_kernel(
+    ep_size,
+    tokens,
+    norm_gain,
+    expert_ids,
+    route_weights,
+    gate_hbm,
+    up_hbm,
+    down_hbm,
+    final_gain,
+    out,
+    rows_all,
+    gate_w,
+    up_w,
+    down_w,
+    normed,
+    gains,
+    table,
+    tables,
+    own,
+    pair_out,
+    pair_in,
+    diag_out,
+    x_out,
+    y_out,
+    z_out,
+    diag_x,
+    diag_y,
+    x_in,
+    y_in,
+    z_in,
+    home,
+    square_out,
+    squares_in,
+    weight_sem,
+    send_sem,
+    recv_sem,
+):
+    groups = ep_size // 2
+    tok, width = tokens.shape
+    half = tok // 2
+    model_width = 4 * width
+    e, t = lax.axis_index("ep"), lax.axis_index("tp")
+    z, x, y, c = e // 2, e % 2, t // 2, t % 2
+
+    def device(zz, xx, yy, cc):
+        return (zz * 2 + xx, yy * 2 + cc)
+
+    x_peer, y_peer, c_peer = device(z, 1 - x, y, c), device(z, x, 1 - y, c), device(z, x, y, 1 - c)
+    tp_peers = {(1, 0): y_peer, (0, 1): c_peer, (1, 1): device(z, x, 1 - y, 1 - c)}
+    ep_peers = {
+        (dz, dx): device((z + dz) % groups, (x + dx) % 2, y, c)
+        for dz in range(groups)
+        for dx in range(2)
+        if dz or dx
+    }
+
+    loads = [
+        pltpu.make_async_copy(src.at[0], dst, weight_sem.at[i])
+        for i, (src, dst) in enumerate(((gate_hbm, gate_w), (up_hbm, up_w), (down_hbm, down_w)))
+    ]
+    for load in loads:
+        load.start()
+
+    barrier = pltpu.get_barrier_semaphore()
+    peers = list(tp_peers.values()) + list(ep_peers.values())
+    for peer in peers:
+        pl.semaphore_signal(barrier, inc=1, device_id=peer, device_id_type=MESH)
+
+    lanes = lax.broadcasted_iota(jnp.int32, (tok, 128), 1)
+    dense = jnp.zeros((tok, 128), jnp.float32)
+    for k in range(expert_ids.shape[1]):
+        dense = dense + jnp.where(
+            expert_ids[:, k : k + 1] == lanes, route_weights[:, k : k + 1], 0.0
+        )
+    table[...] = jnp.transpose(dense)[:ep_size]
+    tables[e] = table[...]
+    gains[t] = norm_gain[...]
+    rows_all[z, t, x] = tokens[...]
+    pl.semaphore_wait(barrier, len(peers))
+
+    sent = []
+
+    def remote(src, dst, slot, peer):
+        return pltpu.make_async_remote_copy(
+            src_ref=src,
+            dst_ref=dst,
+            send_sem=send_sem.at[slot],
+            recv_sem=recv_sem.at[slot],
+            device_id=peer,
+            device_id_type=MESH,
+        )
+
+    def send(src, dst, slot, peer):
+        copy = remote(src, dst, slot, peer)
+        copy.start()
+        sent.append(copy)
+
+    def arrived(dst, slot):
+        remote(dst, dst, slot, c_peer).wait_recv()
+
+    def block(g, xx, yy, cc):
+        return rows_all.at[(z + g) % groups, yy * 2 + cc, xx]
+
+    small = groups * PER_GROUP
+
+    def gather_z(g):
+        if g:
+            arrived(block(g, x, y, c), g * PER_GROUP)
+        src = block(g, x, y, c) if g else tokens
+        dst = block(g, x, y, c)
+        send(src, dst, g * PER_GROUP + 1, x_peer)
+        send(src, dst, g * PER_GROUP + 2, y_peer)
+        send(src, dst, g * PER_GROUP + 3, c_peer)
+
+    def gather_xy(g):
+        base = g * PER_GROUP
+        from_x = block(g, 1 - x, y, c)
+        arrived(from_x, base + 1)
+        send(from_x.at[pl.ds(0, half)], from_x.at[pl.ds(0, half)], base + 7, y_peer)
+        send(from_x, from_x, base + 4, c_peer)
+        from_y = block(g, x, 1 - y, c)
+        arrived(from_y, base + 2)
+        send(from_y.at[pl.ds(half, half)], from_y.at[pl.ds(half, half)], base + 8, x_peer)
+        send(from_y, from_y, base + 5, c_peer)
+
+    def gather_diag(g):
+        base = g * PER_GROUP
+        far = block(g, 1 - x, 1 - y, c)
+        arrived(far.at[pl.ds(0, half)], base + 7)
+        arrived(far.at[pl.ds(half, half)], base + 8)
+        send(far, far, base + 6, c_peer)
+
+    def compute(g):
+        base = g * PER_GROUP
+        arrived(block(g, x, y, 1 - c), base + 3)
+        arrived(block(g, 1 - x, y, 1 - c), base + 4)
+        arrived(block(g, x, 1 - y, 1 - c), base + 5)
+        arrived(block(g, 1 - x, 1 - y, 1 - c), base + 6)
+        zz = (z + g) % groups
+        squares = jnp.zeros((2 * tok, 1), jnp.float32)
+        for s in range(4):
+            v = rows_all[zz, s].reshape(2 * tok, width).astype(jnp.float32)
+            squares = squares + jnp.sum(v * v, axis=1, keepdims=True)
+        scale = lax.rsqrt(squares / model_width + EPSILON)
+        for s in range(4):
+            v = rows_all[zz, s].reshape(2 * tok, width).astype(jnp.float32)
+            normed[:, s * width : (s + 1) * width] = (v * scale * gains[s]).astype(jnp.bfloat16)
+        columns = [
+            jnp.transpose(jnp.broadcast_to(tables[zz * 2 + xx, pl.ds(e, 1), :], (8, tok)))[:, :1]
+            for xx in range(2)
+        ]
+        share = jnp.concatenate(columns, axis=0)
+        lhs = normed[...]
+        gate_pre = jnp.minimum(
+            jnp.dot(lhs, gate_w[...], preferred_element_type=jnp.float32), CLAMP_LIMIT
+        )
+        up_pre = jnp.clip(
+            jnp.dot(lhs, up_w[...], preferred_element_type=jnp.float32), -CLAMP_LIMIT, CLAMP_LIMIT
+        )
+        activated = (
+            (up_pre + 1.0) * gate_pre * jax.nn.sigmoid(SIGMOID_SLOPE * gate_pre) * share
+        ).astype(jnp.bfloat16)
+
+        def project(j, cc):
+            yy = y if j == 0 else 1 - y
+            start = pl.multiple_of((yy * 2 + cc) * width, width)
+            value = jnp.dot(
+                activated, down_w[:, pl.ds(start, width)], preferred_element_type=jnp.float32
+            )
+            return value.reshape(2, tok, width)
+
+        for j in range(2):
+            pair_out[g, j] = project(j, 1 - c).astype(jnp.bfloat16)
+        send(pair_out.at[g], pair_in.at[g], base + 9, c_peer)
+        for j in range(2):
+            own[g, j] = project(j, c)
+
+    def pair_sum(g, j, xx, start, count):
+        rows = pl.ds(start, count)
+        return own[g, j, xx, rows, :] + pair_in[g, j, xx, rows, :].astype(jnp.float32)
+
+    low, high = pl.ds(0, half), pl.ds(half, half)
+
+    def reduce_first(g):
+        base = g * PER_GROUP
+        arrived(pair_in.at[g], base + 9)
+        diag_out[g] = pair_sum(g, 1, 1 - x, 0, tok).astype(jnp.bfloat16)
+        send(diag_out.at[g, low], diag_x.at[g], base + 10, x_peer)
+        send(diag_out.at[g, high], diag_y.at[g], base + 11, y_peer)
+        x_out[g, low] = pair_sum(g, 0, 1 - x, 0, half).astype(jnp.bfloat16)
+        send(x_out.at[g, low], x_in.at[g, low], base + 12, x_peer)
+        y_out[g, high] = pair_sum(g, 1, x, half, half).astype(jnp.bfloat16)
+        send(y_out.at[g, high], y_in.at[g, high], base + 13, y_peer)
+
+    def reduce_second(g):
+        base = g * PER_GROUP
+        arrived(diag_x.at[g], base + 10)
+        y_out[g, low] = (
+            pair_sum(g, 1, x, 0, half) + diag_x[g].astype(jnp.float32)
+        ).astype(jnp.bfloat16)
+        send(y_out.at[g, low], y_in.at[g, low], base + 14, y_peer)
+        arrived(diag_y.at[g], base + 11)
+        x_out[g, high] = (
+            pair_sum(g, 0, 1 - x, half, half) + diag_y[g].astype(jnp.float32)
+        ).astype(jnp.bfloat16)
+        send(x_out.at[g, high], x_in.at[g, high], base + 15, x_peer)
+
+    def reduce_third(g):
+        base = g * PER_GROUP
+        arrived(x_in.at[g, low], base + 12)
+        arrived(y_in.at[g, high], base + 13)
+        arrived(y_in.at[g, low], base + 14)
+        arrived(x_in.at[g, high], base + 15)
+        total = (
+            pair_sum(g, 0, x, 0, tok) + x_in[g].astype(jnp.float32) + y_in[g].astype(jnp.float32)
+        )
+        if g:
+            back = groups - g
+            z_out[g] = total.astype(jnp.bfloat16)
+            send(
+                z_out.at[g],
+                z_in.at[back],
+                back * PER_GROUP + 16,
+                device((z + g) % groups, x, y, c),
+            )
+        else:
+            home[...] = total
+
+    order = sorted(range(groups), key=lambda g: min(g, groups - g))
+
+    for g in order[1:]:
+        back = groups - g
+        send(tokens, block(0, x, y, c), back * PER_GROUP, device((z + g) % groups, x, y, c))
+    gather_z(0)
+    for (dy, dc), peer in tp_peers.items():
+        send(norm_gain, gains.at[t], small + ep_size + dy * 2 + dc, peer)
+    for (dz, dx), peer in ep_peers.items():
+        send(table, tables.at[e], small + ((groups - dz) % groups) * 2 + dx, peer)
+
+    if groups > 1:
+        gather_z(order[1])
+    gather_xy(0)
+    for i, g in enumerate(order):
+        if i + 2 < groups:
+            gather_z(order[i + 2])
+        if i + 1 < groups:
+            gather_xy(order[i + 1])
+        gather_diag(g)
+        if i == 0:
+            for dy, dc in tp_peers:
+                arrived(gains.at[t], small + ep_size + dy * 2 + dc)
+            for dz, dx in ep_peers:
+                arrived(tables.at[e], small + dz * 2 + dx)
+            for load in loads:
+                load.wait()
+        else:
+            reduce_first(order[i - 1])
+        compute(g)
+        if i >= 1:
+            reduce_second(order[i - 1])
+        if i >= 2:
+            reduce_third(order[i - 2])
+    reduce_first(order[-1])
+    if groups > 1:
+        reduce_third(order[-2])
+    reduce_second(order[-1])
+    reduce_third(order[-1])
+
+    mixture = home[...]
+    for g in order[1:]:
+        arrived(z_in.at[g], g * PER_GROUP + 16)
+        mixture = mixture + z_in[g].astype(jnp.float32)
+    partial_squares = jnp.sum(mixture * mixture, axis=1, keepdims=True)
+    square_out[...] = jnp.transpose(jnp.broadcast_to(partial_squares, (tok, 128)))[:8]
+    squares = square_out[...]
+    for (dy, dc), peer in tp_peers.items():
+        send(square_out, squares_in.at[dy * 2 + dc], small + ep_size + 4 + dy * 2 + dc, peer)
+    for dy, dc in tp_peers:
+        arrived(squares_in.at[dy * 2 + dc], small + ep_size + 4 + dy * 2 + dc)
+        squares = squares + squares_in[dy * 2 + dc]
+    scale = lax.rsqrt(jnp.transpose(squares)[:, :1] / model_width + EPSILON)
+    out[...] = (mixture * scale * final_gain[...]).astype(jnp.bfloat16)
+    for copy in sent:
+        copy.wait_send()
+
+
+def fused_local(
+    ep_size,
+    tokens,
+    norm_gain,
+    expert_ids,
+    route_weights,
+    gate_proj,
+    up_proj,
+    down_proj,
+    final_gain,
+):
+    tok, width = tokens.shape
+    model_width, hidden = gate_proj.shape[1:]
+    groups = ep_size // 2
+    half = tok // 2
+    bf16, f32 = jnp.bfloat16, jnp.float32
+    slots = groups * PER_GROUP + ep_size + 8
+    vmem = pl.BlockSpec(memory_space=pltpu.VMEM)
+    hbm = pl.BlockSpec(memory_space=pl.ANY)
+    return pl.pallas_call(
+        functools.partial(fused_kernel, ep_size),
+        out_shape=jax.ShapeDtypeStruct((tok, width), bf16),
+        in_specs=[vmem] * 4 + [hbm] * 3 + [vmem],
+        out_specs=vmem,
+        scratch_shapes=[
+            pltpu.VMEM((groups, 4, 2, tok, width), bf16),
+            pltpu.VMEM((model_width, hidden), bf16),
+            pltpu.VMEM((model_width, hidden), bf16),
+            pltpu.VMEM((hidden, model_width), bf16),
+            pltpu.VMEM((2 * tok, model_width), bf16),
+            pltpu.VMEM((4, 1, width), f32),
+            pltpu.VMEM((ep_size, tok), f32),
+            pltpu.VMEM((ep_size, ep_size, tok), f32),
+            pltpu.VMEM((groups, 2, 2, tok, width), f32),
+            pltpu.VMEM((groups, 2, 2, tok, width), bf16),
+            pltpu.VMEM((groups, 2, 2, tok, width), bf16),
+            pltpu.VMEM((groups, tok, width), bf16),
+            pltpu.VMEM((groups, tok, width), bf16),
+            pltpu.VMEM((groups, tok, width), bf16),
+            pltpu.VMEM((groups, tok, width), bf16),
+            pltpu.VMEM((groups, half, width), bf16),
+            pltpu.VMEM((groups, half, width), bf16),
+            pltpu.VMEM((groups, tok, width), bf16),
+            pltpu.VMEM((groups, tok, width), bf16),
+            pltpu.VMEM((groups, tok, width), bf16),
+            pltpu.VMEM((tok, width), f32),
+            pltpu.VMEM((8, tok), f32),
+            pltpu.VMEM((4, 8, tok), f32),
+            pltpu.SemaphoreType.DMA((3,)),
+            pltpu.SemaphoreType.DMA((slots,)),
+            pltpu.SemaphoreType.DMA((slots,)),
+        ],
+        compiler_params=pltpu.CompilerParams(
+            collective_id=0, has_side_effects=True, vmem_limit_bytes=48 * 1024 * 1024
+        ),
+    )(
+        tokens,
+        norm_gain[None, :],
+        expert_ids,
+        route_weights,
+        gate_proj,
+        up_proj,
+        down_proj,
+        final_gain[None, :],
+    )
+
+
 def solution(mesh):
     placed = (
         P("ep", "tp"),
@@ -85,6 +445,13 @@
         P("ep", "tp", None),
         P("tp"),
     )
+    def step(*args):
+        tok_rows, choose_count = args[2].shape
+        capacity = min(tok_rows, 2 * tok_rows * choose_count // mesh.shape["ep"])
+        if capacity == tok_rows and mesh.shape["tp"] == 4 and mesh.shape["ep"] % 2 == 0:
+            return fused_local(mesh.shape["ep"], *args)
+        return local(*args)
+
     return jax.shard_map(
-        local, mesh=mesh, in_specs=placed, out_specs=P("ep", "tp"), check_vma=False
-    )
+        step, mesh=mesh, in_specs=placed, out_specs=P("ep", "tp"), check_vma=False
+    )

time: 134 us -> 52.1 us (0.39)
  waiting for transfers between devices: 67.4 us -> 0 us
  Pallas kernels: 0 us -> 44.2 us
  blocking collectives: 33.3 us -> 0 us
  between operations: 13.5 us -> 0.02 us
  matrix products: 11.4 us -> 0 us
  local copies, waits for them, and re-layouts: 0.16 us -> 7.55 us
  starting transfers between devices: 5.56 us -> 0 us
  other arithmetic: 2.65 us -> 0 us
    pallas_call x0 -> x1, Pallas kernels: none -> 44.2 us  [fused_local(): pl.pallas_call(functools.partial(fused_kernel, ep_size), out_shape=jax.Sh...]
    reduce_scatter x1 -> x0, waiting for transfers between devices: 31.3 us -> none  [local(): lax.psum_scatter(partial_value.astype(jnp.bfloat16), 'tp', scatter_dimens...]
    all_gather x1 -> x0, waiting for transfers between devices: 21.8 us -> none  [local(): lax.all_gather(lax.all_to_all(outbound, 'ep', split_axis=0, concat_axis=0...]
    all_to_all x1 -> x0, blocking collectives: 19 us -> none  [local(): lax.all_to_all(outbound, 'ep', split_axis=0, concat_axis=0, tiled=True)]
    psum x2 -> x0, blocking collectives: 14.3 us -> none  [the longest x1 8.4 us: local(): squares = lax.psum(jnp.sum(input_rows * input_rows, axis=1), 'tp')]
    all_to_all x1 -> x0, waiting for transfers between devices: 14.3 us -> none  [local(): lax.all_to_all(expert_out, 'ep', split_axis=0, concat_axis=0, tiled=True)]
    dot_general x4 -> x0, matrix products: 11.4 us -> none  [the longest x1 6.02 us: expert_partial(): return jnp.dot(activated, down_proj[0], preferred_element_type=jnp.float32)]
    unnamed x8 -> x13, local copies, waits for them, and re-layouts: 0.02 us -> 7.55 us
  transfers between devices with their start and end apart: 3 -> 0, of which waited for: 3 -> 0; matrix products, arithmetic and copies ran while one was open for 0% -> 0% of each run, Pallas kernels for 0% -> 0%
where the time goes in v1:
time: 52.1 us; the launch traced here: 51.7 us
  Pallas kernels  44.2 us (85%)
  local copies, waits for them, and re-layouts  7.55 us (14%)
    pallas_call x1, Pallas kernels, fused_local(): pl.pallas_call(functools.partial(fused_kernel, ep_size), out_shape=jax.Sh...  44.2 us
    unnamed x13, local copies, waits for them, and re-layouts  7.55 us

profile of v1, /device:TPU:0, one launch (start us, length us, event | category | flops | bytes accessed | tf_op | source)
XLA Modules:
  0.0 51.7 jit_solution(5465212118526608284)
XLA Ops:
  0.0 0.8 %copy.9.expert_ids = s32[64,4]{1,0:T(8,128)S(1)} copy(s32[64,4]{0,1:T(4,128)} %param.10) | data formatting | bytes 2048 | tf_op args[2]
  0.8 0.8 %copy.10.route_weights = f32[64,4]{1,0:T(8,128)S(1)} copy(f32[64,4]{0,1:T(4,128)} %param.11) | data formatting | bytes 2048 | tf_op args[3]
  1.5 0.0 copy-start
  1.5 1.6 %copy-done = bf16[1,2048,512]{2,1,0:T(8,128)(2,1)S(1)} copy-done((bf16[1,2048,512]{2,1,0:T(8,128)(2,1)S(1)}, bf16[1,2048,512]{2,1,0:T(8,128)(2,1)}, u32[]{:S(2)}) %copy-start) | copy-done | bytes 2097176
  3.1 0.0 copy-start.1
  3.1 1.6 %copy-done.1 = bf16[1,2048,512]{2,1,0:T(8,128)(2,1)S(1)} copy-done((bf16[1,2048,512]{2,1,0:T(8,128)(2,1)S(1)}, bf16[1,2048,512]{2,1,0:T(8,128)(2,1)}, u32[]{:S(2)}) %copy-start.1) | copy-done | bytes 2097176
  4.7 0.0 copy-start.2
  4.7 0.8 %copy-done.2 = bf16[64,512]{1,0:T(8,128)(2,1)S(1)} copy-done((bf16[64,512]{1,0:T(8,128)(2,1)S(1)}, bf16[64,512]{1,0:T(8,128)(2,1)}, u32[]{:S(2)}) %copy-start.2) | copy-done | bytes 65560
  5.6 0.0 copy-start.3
  5.6 0.7 %copy-done.3 = f32[512]{0:T(512)S(1)} copy-done((f32[512]{0:T(512)S(1)}, f32[512]{0:T(512)}, u32[]{:S(2)}) %copy-start.3) | copy-done | bytes 2072
  6.2 0.0 copy-start.4
  6.2 0.7 %copy-done.4 = f32[512]{0:T(512)S(1)} copy-done((f32[512]{0:T(512)S(1)}, f32[512]{0:T(512)}, u32[]{:S(2)}) %copy-start.4) | copy-done | bytes 2072
  6.9 44.2 %shard_map.82 = bf16[64,512]{1,0:T(8,128)(2,1)S(1)} custom-call(bf16[64,512]{1,0:T(8,128)(2,1)S(1)} %copy-done.2, f32[1,512]{1,0:T(1,128)S(1)} %bitcast.2, s32[64,4]{1,0:T(8,128)S(1)} %copy.9.expert_ids, f32[64,4]{1,0:T(8,128)S(1)} %copy.10.route_weights, bf16[1,2048,512]{2,1,0:T(8,128)(2,1)S(1)} %copy-done, bf16[1,2048,512]{2,1,0:T(8,128)(2,1)S(1)} %copy-done.1, ...), custom_call_target="tpu_custom_call" | custom-call | tf_op jit(solution)/shard_map/pallas_call | solution.py:389
  51.1 0.6 %copy.12 = bf16[64,512]{1,0:T(8,128)(2,1)} copy(bf16[64,512]{1,0:T(8,128)(2,1)S(1)} %shard_map.82) | data formatting | bytes 131072
Async XLA Ops:
  1.5 1.6 %copy-start = (bf16[1,2048,512]{2,1,0:T(8,128)(2,1)S(1)}, bf16[1,2048,512]{2,1,0:T(8,128)(2,1)}, u32[]{:S(2)}) copy-start(bf16[1,2048,512]{2,1,0:T(8,128)(2,1)} %gate_hbm.1) | copy-start | bytes 6291460
  3.1 1.6 %copy-start.1 = (bf16[1,2048,512]{2,1,0:T(8,128)(2,1)S(1)}, bf16[1,2048,512]{2,1,0:T(8,128)(2,1)}, u32[]{:S(2)}) copy-start(bf16[1,2048,512]{2,1,0:T(8,128)(2,1)} %up_hbm.1) | copy-start | bytes 6291460
  4.7 0.8 %copy-start.2 = (bf16[64,512]{1,0:T(8,128)(2,1)S(1)}, bf16[64,512]{1,0:T(8,128)(2,1)}, u32[]{:S(2)}) copy-start(bf16[64,512]{1,0:T(8,128)(2,1)} %tokens.1) | copy-start | bytes 196612
  5.6 0.7 %copy-start.3 = (f32[512]{0:T(512)S(1)}, f32[512]{0:T(512)}, u32[]{:S(2)}) copy-start(f32[512]{0:T(512)} %param.9) | copy-start | bytes 6148
  6.2 0.7 %copy-start.4 = (f32[512]{0:T(512)S(1)}, f32[512]{0:T(512)}, u32[]{:S(2)}) copy-start(f32[512]{0:T(512)} %param.15) | copy-start | bytes 6148

commit v2 on v1

--- a/solution.py
+++ b/solution.py
@@ -80,22 +80,35 @@
     ).astype(jnp.bfloat16)
 
 
+def stage_plan(groups):
+    plan = [("z", 1), ("x", 0), ("z", 2), ("g", 0), ("x", 1), ("d", 0)]
+    for i in range(groups):
+        plan += [("z", i + 3), ("x", i + 2), ("u", i), ("d", i + 1), ("v", i)]
+        plan += [("1", i - 1), ("2", i - 2), ("3", i - 3)]
+    last = groups - 1
+    plan += [("1", last), ("2", last - 1), ("3", last - 2), ("2", last), ("3", last - 1), ("3", last)]
+    return [(kind, place) for kind, place in plan if 0 <= place < groups]
+
+
 def fused_kernel(
     ep_size,
-    tokens,
-    norm_gain,
-    expert_ids,
-    route_weights,
+    tokens_hbm,
+    gain_hbm,
+    ids_hbm,
+    route_hbm,
     gate_hbm,
     up_hbm,
     down_hbm,
-    final_gain,
+    final_hbm,
     out,
     rows_all,
+    expert_ids,
+    route_weights,
+    final_gain,
     gate_w,
     up_w,
     down_w,
-    normed,
+    hidden_act,
     gains,
     table,
     tables,
@@ -119,7 +132,7 @@
     recv_sem,
 ):
     groups = ep_size // 2
-    tok, width = tokens.shape
+    tok, width = tokens_hbm.shape
     half = tok // 2
     model_width = 4 * width
     e, t = lax.axis_index("ep"), lax.axis_index("tp")
@@ -138,8 +151,19 @@
     }
 
     loads = [
-        pltpu.make_async_copy(src.at[0], dst, weight_sem.at[i])
-        for i, (src, dst) in enumerate(((gate_hbm, gate_w), (up_hbm, up_w), (down_hbm, down_w)))
+        pltpu.make_async_copy(src, dst, weight_sem.at[i])
+        for i, (src, dst) in enumerate(
+            (
+                (tokens_hbm, rows_all.at[z, t, x]),
+                (ids_hbm, expert_ids),
+                (route_hbm, route_weights),
+                (gain_hbm, gains.at[t]),
+                (final_hbm, final_gain),
+                (gate_hbm.at[0], gate_w),
+                (up_hbm.at[0], up_w),
+                (down_hbm.at[0], down_w),
+            )
+        )
     ]
     for load in loads:
         load.start()
@@ -149,16 +173,16 @@
     for peer in peers:
         pl.semaphore_signal(barrier, inc=1, device_id=peer, device_id_type=MESH)
 
-    lanes = lax.broadcasted_iota(jnp.int32, (tok, 128), 1)
-    dense = jnp.zeros((tok, 128), jnp.float32)
-    for k in range(expert_ids.shape[1]):
+    for load in loads[:4]:
+        load.wait()
+    experts = lax.broadcasted_iota(jnp.int32, (ep_size, tok), 0)
+    dense = jnp.zeros((ep_size, tok), jnp.float32)
+    for k in range(expert_ids.shape[0]):
         dense = dense + jnp.where(
-            expert_ids[:, k : k + 1] == lanes, route_weights[:, k : k + 1], 0.0
-        )
-    table[...] = jnp.transpose(dense)[:ep_size]
-    tables[e] = table[...]
-    gains[t] = norm_gain[...]
-    rows_all[z, t, x] = tokens[...]
+            expert_ids[k : k + 1, :] == experts, route_weights[k : k + 1, :], 0.0
+        )
+    table[...] = dense
+    tables[e] = dense
     pl.semaphore_wait(barrier, len(peers))
 
     sent = []
@@ -189,8 +213,7 @@
     def gather_z(g):
         if g:
             arrived(block(g, x, y, c), g * PER_GROUP)
-        src = block(g, x, y, c) if g else tokens
-        dst = block(g, x, y, c)
+        src = dst = block(g, x, y, c)
         send(src, dst, g * PER_GROUP + 1, x_peer)
         send(src, dst, g * PER_GROUP + 2, y_peer)
         send(src, dst, g * PER_GROUP + 3, c_peer)
@@ -213,36 +236,40 @@
         arrived(far.at[pl.ds(half, half)], base + 8)
         send(far, far, base + 6, c_peer)
 
-    def compute(g):
+    def expand(g):
         base = g * PER_GROUP
         arrived(block(g, x, y, 1 - c), base + 3)
         arrived(block(g, 1 - x, y, 1 - c), base + 4)
         arrived(block(g, x, 1 - y, 1 - c), base + 5)
         arrived(block(g, 1 - x, 1 - y, 1 - c), base + 6)
         zz = (z + g) % groups
-        squares = jnp.zeros((2 * tok, 1), jnp.float32)
-        for s in range(4):
-            v = rows_all[zz, s].reshape(2 * tok, width).astype(jnp.float32)
-            squares = squares + jnp.sum(v * v, axis=1, keepdims=True)
-        scale = lax.rsqrt(squares / model_width + EPSILON)
-        for s in range(4):
-            v = rows_all[zz, s].reshape(2 * tok, width).astype(jnp.float32)
-            normed[:, s * width : (s + 1) * width] = (v * scale * gains[s]).astype(jnp.bfloat16)
+        slices = [rows_all[zz, s].reshape(2 * tok, width) for s in range(4)]
+        squares = jnp.zeros((2 * tok, width), jnp.float32)
+        for v in slices:
+            v = v.astype(jnp.float32)
+            squares = squares + v * v
+        scale = lax.rsqrt(jnp.sum(squares, axis=1, keepdims=True) / model_width + EPSILON)
         columns = [
             jnp.transpose(jnp.broadcast_to(tables[zz * 2 + xx, pl.ds(e, 1), :], (8, tok)))[:, :1]
             for xx in range(2)
         ]
         share = jnp.concatenate(columns, axis=0)
-        lhs = normed[...]
+        lhs = jnp.concatenate(slices, axis=1)
         gate_pre = jnp.minimum(
-            jnp.dot(lhs, gate_w[...], preferred_element_type=jnp.float32), CLAMP_LIMIT
+            jnp.dot(lhs, gate_w[...], preferred_element_type=jnp.float32) * scale, CLAMP_LIMIT
         )
         up_pre = jnp.clip(
-            jnp.dot(lhs, up_w[...], preferred_element_type=jnp.float32), -CLAMP_LIMIT, CLAMP_LIMIT
-        )
-        activated = (
+            jnp.dot(lhs, up_w[...], preferred_element_type=jnp.float32) * scale,
+            -CLAMP_LIMIT,
+            CLAMP_LIMIT,
+        )
+        hidden_act[g] = (
             (up_pre + 1.0) * gate_pre * jax.nn.sigmoid(SIGMOID_SLOPE * gate_pre) * share
         ).astype(jnp.bfloat16)
+
+    def contract(g):
+        base = g * PER_GROUP
+        activated = hidden_act[g]
 
         def project(j, cc):
             yy = y if j == 0 else 1 - y
@@ -313,41 +340,41 @@
 
     for g in order[1:]:
         back = groups - g
-        send(tokens, block(0, x, y, c), back * PER_GROUP, device((z + g) % groups, x, y, c))
+        send(block(0, x, y, c), block(0, x, y, c), back * PER_GROUP, device((z + g) % groups, x, y, c))
     gather_z(0)
     for (dy, dc), peer in tp_peers.items():
-        send(norm_gain, gains.at[t], small + ep_size + dy * 2 + dc, peer)
+        send(gains.at[t], gains.at[t], small + ep_size + dy * 2 + dc, peer)
     for (dz, dx), peer in ep_peers.items():
         send(table, tables.at[e], small + ((groups - dz) % groups) * 2 + dx, peer)
 
-    if groups > 1:
-        gather_z(order[1])
-    gather_xy(0)
-    for i, g in enumerate(order):
-        if i + 2 < groups:
-            gather_z(order[i + 2])
-        if i + 1 < groups:
-            gather_xy(order[i + 1])
-        gather_diag(g)
-        if i == 0:
-            for dy, dc in tp_peers:
-                arrived(gains.at[t], small + ep_size + dy * 2 + dc)
-            for dz, dx in ep_peers:
-                arrived(tables.at[e], small + dz * 2 + dx)
-            for load in loads:
-                load.wait()
+    def settle():
+        for dy, dc in tp_peers:
+            arrived(gains.at[t], small + ep_size + dy * 2 + dc)
+        for dz, dx in ep_peers:
+            arrived(tables.at[e], small + dz * 2 + dx)
+        for load in loads[4:]:
+            load.wait()
+        for s in range(4):
+            gain = jnp.transpose(jnp.broadcast_to(gains[s], (8, width)))[:, :1]
+            for w in (gate_w, up_w):
+                part = w[s * width : (s + 1) * width, :].astype(jnp.float32)
+                w[s * width : (s + 1) * width, :] = (part * gain).astype(jnp.bfloat16)
+
+    steps = {
+        "z": gather_z,
+        "x": gather_xy,
+        "d": gather_diag,
+        "u": expand,
+        "v": contract,
+        "1": reduce_first,
+        "2": reduce_second,
+        "3": reduce_third,
+    }
+    for kind, place in stage_plan(groups):
+        if kind == "g":
+            settle()
         else:
-            reduce_first(order[i - 1])
-        compute(g)
-        if i >= 1:
-            reduce_second(order[i - 1])
-        if i >= 2:
-            reduce_third(order[i - 2])
-    reduce_first(order[-1])
-    if groups > 1:
-        reduce_third(order[-2])
-    reduce_second(order[-1])
-    reduce_third(order[-1])
+            steps[kind](order[place])
 
     mixture = home[...]
     for g in order[1:]:
@@ -385,18 +412,21 @@
     bf16, f32 = jnp.bfloat16, jnp.float32
     slots = groups * PER_GROUP + ep_size + 8
     vmem = pl.BlockSpec(memory_space=pltpu.VMEM)
-    hbm = pl.BlockSpec(memory_space=pl.ANY)
+    hbm = pl.BlockSpec(memory_space=pltpu.HBM)
     return pl.pallas_call(
         functools.partial(fused_kernel, ep_size),
         out_shape=jax.ShapeDtypeStruct((tok, width), bf16),
-        in_specs=[vmem] * 4 + [hbm] * 3 + [vmem],
+        in_specs=[hbm] * 8,
         out_specs=vmem,
         scratch_shapes=[
             pltpu.VMEM((groups, 4, 2, tok, width), bf16),
+            pltpu.VMEM((expert_ids.shape[1], tok), jnp.int32),
+            pltpu.VMEM((expert_ids.shape[1], tok), f32),
+            pltpu.VMEM((1, width), f32),
             pltpu.VMEM((model_width, hidden), bf16),
             pltpu.VMEM((model_width, hidden), bf16),
             pltpu.VMEM((hidden, model_width), bf16),
-            pltpu.VMEM((2 * tok, model_width), bf16),
+            pltpu.VMEM((groups, 2 * tok, hidden), bf16),
             pltpu.VMEM((4, 1, width), f32),
             pltpu.VMEM((ep_size, tok), f32),
             pltpu.VMEM((ep_size, ep_size, tok), f32),
@@ -415,18 +445,18 @@
             pltpu.VMEM((tok, width), f32),
             pltpu.VMEM((8, tok), f32),
             pltpu.VMEM((4, 8, tok), f32),
-            pltpu.SemaphoreType.DMA((3,)),
+            pltpu.SemaphoreType.DMA((8,)),
             pltpu.SemaphoreType.DMA((slots,)),
             pltpu.SemaphoreType.DMA((slots,)),
         ],
         compiler_params=pltpu.CompilerParams(
-            collective_id=0, has_side_effects=True, vmem_limit_bytes=48 * 1024 * 1024
+            collective_id=0, has_side_effects=True, vmem_limit_bytes=67043328
         ),
     )(
         tokens,
         norm_gain[None, :],
-        expert_ids,
-        route_weights,
+        expert_ids.T,
+        route_weights.T,
         gate_proj,
         up_proj,
         down_proj,

time: 52.1 us -> 44 us (0.84)
  local copies, waits for them, and re-layouts: 7.55 us -> 1.47 us
  Pallas kernels: 44.2 us -> 42.3 us
    unnamed x13 -> x1, local copies, waits for them, and re-layouts: 7.55 us -> 1.47 us
    pallas_call x1, Pallas kernels: 44.2 us -> 42.3 us  [fused_local(): pl.pallas_call(functools.partial(fused_kernel, ep_size), out_shape=jax.Sh...]
where the time goes in v2:
time: 44 us; the launch traced here: 43.8 us
  Pallas kernels  42.3 us (96%)
  local copies, waits for them, and re-layouts  1.47 us (3%)
    pallas_call x1, Pallas kernels, fused_local(): pl.pallas_call(functools.partial(fused_kernel, ep_size), out_shape=jax.Sh...  42.3 us
    unnamed x1, local copies, waits for them, and re-layouts  1.47 us

profile of v2, /device:TPU:0, one launch (start us, length us, event | category | flops | bytes accessed | tf_op | source)
XLA Modules:
  0.0 43.8 jit_solution(16540226104334208880)
XLA Ops:
  0.0 42.3 %shard_map.82 = bf16[64,512]{1,0:T(8,128)(2,1)} custom-call(bf16[64,512]{1,0:T(8,128)(2,1)} %tokens_hbm.1, f32[1,512]{1,0:T(1,128)} %bitcast.4, s32[4,64]{1,0:T(4,128)} %bitcast.5, f32[4,64]{1,0:T(4,128)} %bitcast.6, bf16[1,2048,512]{2,1,0:T(8,128)(2,1)} %gate_hbm.1, bf16[1,2048,512]{2,1,0:T(8,128)(2,1)} %up_hbm.1, bf16[1,512,2048]{2,1,0:T(8,128)(2,1)} %down_hbm.1, ...), custom_call_target="tpu_custom_call" | custom-call | tf_op jit(solution)/shard_map/pallas_call | solution.py:416
  42.3 1.5 %copy.10 = bf16[64,512]{1,0:T(8,128)(2,1)} copy(bf16[64,512]{1,0:T(8,128)(2,1)} %shard_map.82) | data formatting | bytes 131072
